TPU v7x, 32 devices: a whole 2x2x4 slice. The times are simulated.
32 devices in a mesh: ep: 16 (over z, y, x), tp: 2 (over core).
Axes of the slice: x: 2, y: 2, z: 4, core: 2. Of those that a mesh axis runs over, the one named last changes fastest.
Arguments:
- tokens: bfloat16 [256, 2048], P('ep'), may hold values from -6 to 6
- recurrent_state: float32 [256, 4, 128, 256], P('ep', 'tp'), may hold values from -6 to 6
- query_weight: bfloat16 [2048, 512], P(None, 'tp'), may hold values from -0.125 to 0.125
- key_weight: bfloat16 [2048, 512], P(None, 'tp'), may hold values from -0.125 to 0.125
- decay_weight: bfloat16 [2048, 512], P(None, 'tp'), may hold values from -0.5 to 0.5
- value_weight: bfloat16 [2048, 1024], P(None, 'tp'), may hold values from -0.125 to 0.125
- gate_weight: bfloat16 [2048, 1024], P(None, 'tp'), may hold values from -0.125 to 0.125
- head_gain: float32 [256], replicated, may hold values from 0.1 to 1.9
- output_weight: bfloat16 [1024, 2048], P('tp'), may hold values from -0.375 to 0.375
- norm_gain: float32 [2, 2048], replicated, may hold values from 0.1 to 1.9
- norm_bias: float32 [2, 2048], replicated, may hold values from -1.8 to 1.8
- group_router: bfloat16 [2048, 4], replicated, may hold values from -0.125 to 0.125
- router_weight: bfloat16 [2048, 32], replicated, may hold values from -0.125 to 0.125
- routes: int32 [256, 2], P('ep'), may hold values from 0 to 31, as said below
- expert_gate: bfloat16 [32, 2048, 256], P(('ep', 'tp')), may hold values from -0.125 to 0.125
- expert_up: bfloat16 [32, 2048, 256], P(('ep', 'tp')), may hold values from -0.125 to 0.125
- expert_down: bfloat16 [32, 256, 2048], P(('ep', 'tp')), may hold values from -1.5 to 1.5
Outputs:
- new_tokens: bfloat16 [256, 2048], P('ep', 'tp')
- new_state: float32 [256, 4, 128, 256], P('ep', 'tp')
Inputs may be any that keep to these rules, and one draw needn't show every extreme that they name: `routes`: each row names two different experts of one group (group g holds the experts g * 8 to g * 8 + 7). In the rows of one device each group is named by the same number of rows and no expert by more than 2 rows; some expert is named by exactly 2 rows of every device.
All inputs are finite; a program needn't handle non-finite values.
Results may differ from a plain program's by a relative error of at most 0.01.
Values may be sent and summed in bfloat16 or wider, within the bound.
A program may use at most 128 MiB of HBM per device.

v0:
```python
import jax
import jax.numpy as jnp
from jax import lax
from jax.sharding import PartitionSpec as P

alpha_res = 2.0**0.5
eps_norm = 1e-05


def layer_normed(inputs, gain_row, bias_row):
    centered = inputs - jnp.mean(inputs, axis=-1, keepdims=True)
    spread = jnp.mean(centered * centered, axis=-1, keepdims=True)
    return centered * lax.rsqrt(spread + eps_norm) * gain_row + bias_row


def on_device(
    tokens,
    recurrent_state,
    query_weight,
    key_weight,
    decay_weight,
    value_weight,
    gate_weight,
    head_gain,
    output_weight,
    norm_gain,
    norm_bias,
    group_router,
    router_weight,
    routes,
    expert_gate,
    expert_up,
    expert_down,
):
    row_count, model_width = tokens.shape
    heads_here = recurrent_state.shape[1]
    key_dim = recurrent_state.shape[2]
    value_dim = recurrent_state.shape[3]

    def project(weight):
        return jnp.dot(tokens, weight, preferred_element_type=jnp.float32)

    queries = project(query_weight).reshape(row_count, heads_here, key_dim) * key_dim ** (-0.5)
    key_rows = project(key_weight).reshape(row_count, heads_here, key_dim)
    value_rows = project(value_weight).reshape(row_count, heads_here, value_dim)
    gate_rows = project(gate_weight)
    decay_rate = jnp.exp(jax.nn.log_sigmoid(project(decay_weight)) / 16.0).reshape(
        row_count, heads_here, key_dim
    )
    new_state = (
        decay_rate[..., None] * recurrent_state + key_rows[..., None] * value_rows[:, :, None, :]
    )
    readout = jnp.sum(queries[..., None] * new_state, axis=2)
    norm_scale = lax.rsqrt(jnp.mean(readout * readout, axis=-1, keepdims=True) + eps_norm)
    gated_rows = (
        (readout * norm_scale * head_gain).reshape(row_count, heads_here * value_dim)
        * jax.nn.silu(gate_rows)
    ).astype(jnp.bfloat16)
    partial_value = jnp.dot(gated_rows, output_weight, preferred_element_type=jnp.float32)
    mixed_sum = lax.psum(partial_value.astype(jnp.bfloat16), "tp").astype(jnp.float32)
    hidden = layer_normed(
        alpha_res * tokens.astype(jnp.float32) + mixed_sum, norm_gain[0], norm_bias[0]
    ).astype(jnp.bfloat16)
    group_count = group_router.shape[1]
    expert_count = router_weight.shape[1]
    per_group = expert_count // group_count
    top_count = routes.shape[1]
    group_logit = jnp.dot(hidden, group_router, preferred_element_type=jnp.float32)
    expert_logit = jnp.dot(hidden, router_weight, preferred_element_type=jnp.float32)
    chosen_group = routes[:, 0] // per_group
    group_hit = chosen_group[:, None] == jnp.arange(group_count, dtype=jnp.int32)[None, :]
    own_logit = jnp.sum(jnp.where(group_hit, group_logit, 0.0), axis=1, keepdims=True)
    group_share = 1.0 / jnp.sum(jnp.exp(group_logit - own_logit), axis=1)
    expert_hit = routes[:, :, None] == jnp.arange(expert_count, dtype=jnp.int32)[None, None, :]
    picked = jnp.sum(jnp.where(expert_hit, expert_logit[:, None, :], 0.0), axis=2)
    route_weight = group_share[:, None] * jax.nn.sigmoid(picked - picked[:, ::-1])
    ep_count = lax.axis_size("ep")
    tp_count = lax.axis_size("tp")
    pair_index = lax.axis_index("tp")
    local_experts = expert_gate.shape[0]
    capacity = 2 * max(1, row_count // expert_count)
    total_slots = expert_count * capacity
    own_slots = total_slots // tp_count
    flat_routes = routes.reshape(row_count * top_count)
    onehot = (flat_routes[:, None] == jnp.arange(expert_count, dtype=jnp.int32)[None, :]).astype(
        jnp.int32
    )
    earlier_count = jnp.sum((jnp.cumsum(onehot, axis=0) - onehot) * onehot, axis=1)
    slot_index = flat_routes * capacity + earlier_count
    pick_all = (slot_index[:, None] == jnp.arange(total_slots, dtype=jnp.int32)[None, :]).astype(
        jnp.bfloat16
    )
    pick_mine = lax.dynamic_slice_in_dim(
        pick_all.reshape(row_count * top_count, ep_count, tp_count, local_experts * capacity),
        pair_index,
        1,
        2,
    ).reshape(row_count * top_count, own_slots)
    outgoing = jnp.einsum(
        "rks,rd->sd",
        pick_mine.reshape(row_count, top_count, own_slots),
        hidden,
        preferred_element_type=jnp.float32,
    ).astype(jnp.bfloat16)
    outgoing = outgoing.reshape(ep_count, local_experts, capacity, model_width)
    col_width = model_width // tp_count
    col_start = pair_index * col_width
    arrived = lax.all_to_all(outgoing, "ep", split_axis=0, concat_axis=0, tiled=True)
    gate_part = jnp.einsum(
        "secd,edf->secf", arrived, expert_gate, preferred_element_type=jnp.float32
    )
    up_part = jnp.einsum("secd,edf->secf", arrived, expert_up, preferred_element_type=jnp.float32)
    activation = (jax.nn.silu(gate_part) * up_part).astype(jnp.bfloat16)
    results = jnp.einsum(
        "secf,efd->secd", activation, expert_down, preferred_element_type=jnp.float32
    ).astype(jnp.bfloat16)
    returned = lax.all_to_all(
        lax.all_to_all(results, "ep", split_axis=0, concat_axis=0, tiled=True),
        "tp",
        split_axis=3,
        concat_axis=1,
        tiled=True,
    )
    fetched = jnp.dot(
        pick_all, returned.reshape(total_slots, col_width), preferred_element_type=jnp.float32
    ).reshape(row_count, top_count, col_width)
    routed_sum = jnp.sum(route_weight[..., None] * fetched, axis=1)
    blended = (
        alpha_res * lax.dynamic_slice_in_dim(hidden, col_start, col_width, 1).astype(jnp.float32)
        + routed_sum
    )
    row_total, row_squares = lax.psum(
        (jnp.sum(blended, axis=1), jnp.sum(blended * blended, axis=1)), "tp"
    )
    row_mean = row_total / model_width
    spread = row_squares / model_width - row_mean * row_mean
    gain_part = lax.dynamic_slice_in_dim(norm_gain[1], col_start, col_width, 0)
    shift_part = lax.dynamic_slice_in_dim(norm_bias[1], col_start, col_width, 0)
    new_tokens = (
        (blended - row_mean[:, None]) * lax.rsqrt(spread[:, None] + eps_norm) * gain_part
        + shift_part
    ).astype(jnp.bfloat16)
    return (new_tokens, new_state)


def solution(mesh):
    in_specs = (
        P("ep", None),
        P("ep", "tp", None, None),
        P(None, "tp"),
        P(None, "tp"),
        P(None, "tp"),
        P(None, "tp"),
        P(None, "tp"),
        P(),
        P("tp", None),
        P(),
        P(),
        P(),
        P(),
        P("ep", None),
        P(("ep", "tp"), None, None),
        P(("ep", "tp"), None, None),
        P(("ep", "tp"), None, None),
    )
    out_specs = (P("ep", "tp"), P("ep", "tp", None, None))
    return jax.shard_map(
        on_device, mesh=mesh, in_specs=in_specs, out_specs=out_specs, check_vma=False
    )
```

profile of v0, /device:TPU:0, one launch (start us, length us, event | category | flops | bytes accessed | tf_op | source)
XLA Modules:
  0.0 94.1 jit_solution(932960176985230560)
XLA Ops:
  7.2 1.7 %convolution_multiply_fusion.1 = f32[16,256]{1,0:T(8,128)S(1)} fusion(bf16[16,2048]{1,0:T(8,128)(2,1)} %param.17, bf16[2048,256]{1,0:T(8,128)(2,1)} %param.19), kind=kOutput, calls=%fused_computation.14 | convolution fusion | flops 16781312 | bytes 1130496 | tf_op jit(solution)/shard_map/dot_general | solution.py:41
  8.9 2.0 %fusion.42 = f32[16,512]{1,0:T(8,128)S(1)} fusion(bf16[16,2048]{1,0:T(8,128)(2,1)} %param.17, bf16[2048,512]{1,0:T(8,128)(2,1)} %param.22), kind=kOutput, calls=%fused_computation.83 | convolution fusion | flops 33554432 | bytes 2195456 | tf_op jit(solution)/shard_map/dot_general | solution.py:41
  11.0 0.2 fusion.41
  11.3 1.5 %fusion.25 = f32[16,256]{1,0:T(8,128)S(1)} fusion(bf16[16,2048]{1,0:T(8,128)(2,1)S(1)} %copy-done.1, bf16[2048,256]{1,0:T(8,128)(2,1)} %param.21), kind=kOutput, calls=%fused_computation.41 | convolution fusion | flops 16814080 | bytes 1130496 | tf_op jit(solution)/shard_map/dot_general | solution.py:41
  12.8 5.7 %multiply_reduce_fusion = (f32[16,2,256]{2,1,0:T(2,128)S(1)}, f32[16,2,128,256]{3,2,1,0:T(8,128)}) fusion(f32[16,2,128]{2,1,0:T(2,128)S(1)} %mul.188, f32[16,2,256]{2,1,0:T(2,128)S(1)} %mul.195, f32[16,2,128]{2,1,0:T(2,128)S(1)} %mul.193, f32[16,2,128,256]{3,2,1,0:T(8,128)} %param.18, f32[16,2,128]{2,1,0:T(2,128)S(1)} %mul.190), kind=kLoop, calls=%fused_computation | loop fusion | flops 5234688 | bytes 8503296 | tf_op jit(solution)/shard_map/reduce_sum | solution.py:53
  18.7 3.0 %convolution_convert_fusion.2 = bf16[16,2048]{1,0:T(8,128)(2,1)} fusion(bf16[512,2048]{1,0:T(8,128)(2,1)S(1)} %copy-done, f32[16,512]{1,0:T(8,128)S(1)} %bitcast.96, f32[512]{0:T(512)S(1)} %bitcast.102, bf16[16,2048]{1,0:T(8,128)(2,1)S(1)} %copy-done.1, bf16[2048,512]{1,0:T(8,128)(2,1)} %param.23), kind=kOutput, calls=%fused_computation.5 | convolution fusion | flops 67198976 | bytes 4360192 | tf_op jit(solution)/shard_map/dot_general | solution.py:59
  21.9 0.6 fusion.34
  23.0 0.8 fusion.10
  23.8 1.1 %reshape.146 = f32[16,2,32]{2,1,0:T(2,128)S(1)} reshape(f32[32,16,1,2]{3,1,0,2:T(8,128)} %fusion.10) | data formatting | bytes 8192 | tf_op jit(solution)/shard_map/rks,rd->sd/convert_element_type | solution.py:99
  25.0 0.6 multiply_add_fusion.3
  25.6 16.7 %all-reduce.3.cloned.1.call-done = bf16[16,2048]{1,0:T(8,128)(2,1)} async-done(((bf16[16,2048]{1,0:T(8,128)(2,1)}), bf16[16,2048]{1,0:T(8,128)(2,1)}) %all-reduce.3.cloned.1.call-update) | async-done | bytes 65552 | tf_op jit(solution)/shard_map/psum | solution.py:60
  42.4 1.0 %fusion.17 = f32[16]{0:T(128)S(1)} fusion(bf16[16,2048]{1,0:T(8,128)(2,1)} %all-reduce.3.cloned.1.call-done, bf16[16,2048]{1,0:T(8,128)(2,1)S(1)} %copy-done.1), kind=kLoop, calls=%fused_computation.27 | loop fusion | flops 163824 | bytes 131136 | tf_op jit(solution)/shard_map/reduce_sum | solution.py:11
  43.3 1.0 %multiply_reduce_fusion.1 = f32[16]{0:T(128)S(1)} fusion(bf16[16,2048]{1,0:T(8,128)(2,1)} %all-reduce.3.cloned.1.call-done, bf16[16,2048]{1,0:T(8,128)(2,1)S(1)} %copy-done.1, f32[16]{0:T(128)S(1)} %broadcast_multiply_fusion.2), kind=kLoop, calls=%fused_computation.23 | loop fusion | flops 229360 | bytes 131200 | tf_op jit(solution)/shard_map/reduce_sum | solution.py:12
  44.4 0.9 add_convert_fusion
  45.3 0.2 fusion.44
  45.5 0.7 reshape.139
  46.3 6.8 %all-to-all-start = ((bf16[16,1,2,2048]{3,2,1,0:T(2,128)(2,1)}), bf16[16,1,2,2048]{3,2,1,0:T(2,128)(2,1)S(1)}, u32[]{:S(2)}, u32[]{:S(2)}) async-start(bf16[16,1,2,2048]{3,2,1,0:T(2,128)(2,1)} %bitcast.4), calls=%async_computation | async-start | bytes 262144 | tf_op jit(solution)/shard_map/all_to_all | solution.py:108
  53.1 0.9 select_reduce_fusion.2
  54.2 6.8 %all-to-all-done = bf16[16,1,2,2048]{3,2,1,0:T(2,128)(2,1)S(1)} async-done(((bf16[16,1,2,2048]{3,2,1,0:T(2,128)(2,1)}), bf16[16,1,2,2048]{3,2,1,0:T(2,128)(2,1)S(1)}, u32[]{:S(2)}, u32[]{:S(2)}) %all-to-all-start) | async-done | bytes 131104 | tf_op jit(solution)/shard_map/all_to_all | solution.py:108
  61.0 1.5 %convolution_bitcast_fusion.1 = f32[16,1,2,256]{3,0,2,1:T(8,128)S(1)} fusion(bf16[1,2048,256]{2,1,0:T(8,128)(2,1)} %param.31, bf16[16,1,2,2048]{3,2,1,0:T(2,128)(2,1)S(1)} %all-to-all-done), kind=kOutput, calls=%fused_computation.10 | convolution fusion | flops 33554432 | bytes 1212416 | tf_op jit(solution)/shard_map/secd,edf->secf/dot_general | solution.py:109
  62.5 2.0 %fusion = bf16[16,1,2,2048]{3,0,2,1:T(8,128)(2,1)S(1)} fusion(bf16[1,256,2048]{2,1,0:T(8,128)(2,1)S(1)} %copy-done.2, bf16[1,2048,256]{2,1,0:T(8,128)(2,1)} %param.32, bf16[16,1,2,2048]{3,2,1,0:T(2,128)(2,1)S(1)} %all-to-all-done, f32[16,1,2,256]{3,0,2,1:T(8,128)S(1)} %convolution_bitcast_fusion.1), kind=kOutput, calls=%fused_computation.4 | convolution fusion | flops 67223552 | bytes 2392064 | tf_op jit(solution)/shard_map/secf,efd->secd/dot_general | solution.py:114
  64.4 0.8 copy.56
  65.2 3.5 %all-to-all-start.1 = ((bf16[16,1,2,2048]{3,2,1,0:T(2,128)(2,1)}), bf16[16,1,2,2048]{3,2,1,0:T(2,128)(2,1)S(1)}, u32[]{:S(2)}, u32[]{:S(2)}) async-start(bf16[16,1,2,2048]{3,2,1,0:T(2,128)(2,1)} %copy.56), calls=%async_computation.1 | async-start | bytes 262144 | tf_op jit(solution)/shard_map/all_to_all | solution.py:118
  69.0 7.6 %all-to-all-done.1 = bf16[16,1,2,2048]{3,2,1,0:T(2,128)(2,1)S(1)} async-done(((bf16[16,1,2,2048]{3,2,1,0:T(2,128)(2,1)}), bf16[16,1,2,2048]{3,2,1,0:T(2,128)(2,1)S(1)}, u32[]{:S(2)}, u32[]{:S(2)}) %all-to-all-start.1) | async-done | bytes 131104 | tf_op jit(solution)/shard_map/all_to_all | solution.py:118
  76.5 0.8 copy.57
  77.3 1.1 %reshape.152 = bf16[2,2,16384]{2,1,0:T(2,128)(2,1)S(1)} reshape(bf16[2048,1,2,16]{3,2,1,0:T(2,128)(2,1)S(1)} %bitcast.93) | data formatting | bytes 262144
  78.4 3.8 %all_to_all.25 = bf16[2,2,16384]{2,1,0:T(2,128)(2,1)S(1)} all-to-all(bf16[2,2,16384]{2,1,0:T(2,128)(2,1)S(1)} %reshape.152), channel_id=1, replica_groups=mesh['ep'=16,'tp'=2] {'tp'}, dimensions={0} | all-to-all | bytes 262144 | tf_op jit(solution)/shard_map/all_to_all | solution.py:117
  82.2 0.7 reshape.153
  82.9 0.8 copy.58
  83.7 0.2 fusion.1
  84.1 2.5 %all-reduce = (f32[16]{0:T(128)S(1)}, f32[16]{0:T(128)S(1)}) all-reduce(f32[16]{0:T(128)S(1)} %get-tuple-element.3, f32[16]{0:T(128)S(1)} %get-tuple-element.2), channel_id=1, replica_groups=mesh['ep'=16,'tp'=2] {'tp'}, use_global_device_ids=true, to_apply=%region_15.16 | all-reduce | flops 32 | bytes 256 | tf_op jit(solution)/shard_map/psum | solution.py:132
  86.6 0.7 add_convert_fusion.1
  (57 shorter events, 1.7 us)
Async XLA Ops:
  7.2 11.5 %copy-start = (bf16[512,2048]{1,0:T(8,128)(2,1)S(1)}, bf16[512,2048]{1,0:T(8,128)(2,1)}, u32[]{:S(2)}) copy-start(bf16[512,2048]{1,0:T(8,128)(2,1)} %param.25) | copy-start | bytes 6291460
  7.2 3.8 %copy-start.1 = (bf16[16,2048]{1,0:T(8,128)(2,1)S(1)}, bf16[16,2048]{1,0:T(8,128)(2,1)}, u32[]{:S(2)}) copy-start(bf16[16,2048]{1,0:T(8,128)(2,1)} %param.17) | copy-start | bytes 196612
  7.2 3.8 %copy-start.3 = (bf16[2048,256]{1,0:T(8,128)(2,1)S(1)}, bf16[2048,256]{1,0:T(8,128)(2,1)}, u32[]{:S(2)}) copy-start(bf16[2048,256]{1,0:T(8,128)(2,1)} %param.20) | copy-start | bytes 3145732
  7.2 35.2 %all-reduce.3.cloned.1.call-start = ((), (), s32[]{:S(2)}) async-start(), calls=%async_computation.3 | async-start | bytes 131072 | tf_op jit(solution)/shard_map/psum | solution.py:60
  12.8 5.9 %copy-start.9 = (f32[256]{0:T(256)S(1)}, f32[256]{0:T(256)}, u32[]{:S(2)}) copy-start(f32[256]{0:T(256)} %param.24) | copy-start | bytes 3076
  18.7 3.1 %copy-start.7 = (s32[16,2]{0,1:T(2,128)S(1)}, s32[16,2]{0,1:T(2,128)}, u32[]{:S(2)}) copy-start(s32[16,2]{0,1:T(2,128)} %param.30) | copy-start | bytes 388
  18.7 4.2 %copy-start.5 = (f32[2,2048]{1,0:T(2,128)S(1)}, f32[2,2048]{1,0:T(2,128)}, u32[]{:S(2)}) copy-start(f32[2,2048]{1,0:T(2,128)} %param.27) | copy-start | bytes 49156
  18.7 4.3 %copy-start.6 = (f32[2,2048]{1,0:T(2,128)S(1)}, f32[2,2048]{1,0:T(2,128)}, u32[]{:S(2)}) copy-start(f32[2,2048]{1,0:T(2,128)} %param.26) | copy-start | bytes 49156
  21.7 32.3 %copy-start.4 = (bf16[2048,32]{0,1:T(8,128)(2,1)S(1)}, bf16[2048,32]{0,1:T(8,128)(2,1)}, u32[]{:S(2)}) copy-start(bf16[2048,32]{0,1:T(8,128)(2,1)} %param.29) | copy-start | bytes 393220
  21.7 40.8 %copy-start.2 = (bf16[1,256,2048]{2,1,0:T(8,128)(2,1)S(1)}, bf16[1,256,2048]{2,1,0:T(8,128)(2,1)}, u32[]{:S(2)}) copy-start(bf16[1,256,2048]{2,1,0:T(8,128)(2,1)} %param.33) | copy-start | bytes 3145732
  46.3 14.7 %all-to-all-start = ((bf16[16,1,2,2048]{3,2,1,0:T(2,128)(2,1)}), bf16[16,1,2,2048]{3,2,1,0:T(2,128)(2,1)S(1)}, u32[]{:S(2)}, u32[]{:S(2)}) async-start(bf16[16,1,2,2048]{3,2,1,0:T(2,128)(2,1)} %bitcast.4), calls=%async_computation | async-start | bytes 262144 | tf_op jit(solution)/shard_map/all_to_all | solution.py:108
  65.2 11.3 %all-to-all-start.1 = ((bf16[16,1,2,2048]{3,2,1,0:T(2,128)(2,1)}), bf16[16,1,2,2048]{3,2,1,0:T(2,128)(2,1)S(1)}, u32[]{:S(2)}, u32[]{:S(2)}) async-start(bf16[16,1,2,2048]{3,2,1,0:T(2,128)(2,1)} %copy.56), calls=%async_computation.1 | async-start | bytes 262144 | tf_op jit(solution)/shard_map/all_to_all | solution.py:118
  77.3 6.5 %copy-start.8 = (s32[16,2]{0,1:T(2,128)S(1)}, s32[16,2]{0,1:T(2,128)}, u32[]{:S(2)}) copy-start(s32[16,2]{0,1:T(2,128)} %multiply_add_fusion.3) | copy-start | bytes 388
Sparse Core Ops, SparseCore 0:
  21.9 20.4 all-reduce.2
where the time goes:
time: 94.9 us; the launch traced here: 94.1 us
  waiting for transfers between devices  31.1 us (33%)
  between operations  14.4 us (15%)
  matrix products  13.3 us (14%)
  other arithmetic  12.1 us (13%)
  starting transfers between devices  10.4 us (11%)
  local copies, waits for them, and re-layouts  6.53 us (7%)
  blocking collectives  6.31 us (7%)
    psum x1, waiting for transfers between devices, on_device(): lax.psum(partial_value.astype(jnp.bfloat16), 'tp').astype(jnp.float32)  16.7 us
    all_to_all x1, waiting for transfers between devices, on_device(): lax.all_to_all(results, 'ep', split_axis=0, concat_axis=0, tiled=True)  7.57 us
    all_to_all x1, starting transfers between devices, on_device(): lax.all_to_all(outgoing, 'ep', split_axis=0, concat_axis=0, tiled=True)  6.83 us
    all_to_all x1, waiting for transfers between devices, on_device(): lax.all_to_all(outgoing, 'ep', split_axis=0, concat_axis=0, tiled=True)  6.8 us
    reduce_sum x1, other arithmetic, on_device(): readout = jnp.sum(queries[..., None] * new_state, axis=2)  5.65 us
    dot_general x4, matrix products, project(): return jnp.dot(tokens, weight, preferred_element_type=jnp.float32)  5.4 us
    all_to_all x1, blocking collectives, on_device(): lax.all_to_all(lax.all_to_all(results, 'ep', split_axis=0, concat_axis=0,...  3.84 us
    all_to_all x1, starting transfers between devices, on_device(): lax.all_to_all(results, 'ep', split_axis=0, concat_axis=0, tiled=True)  3.51 us
  transfers between devices with their start and end apart: 3, of which 3 were waited for; matrix products, arithmetic and copies ran while one was open for 5% of the time, Pallas kernels for 0%

commit v1 on v0

v1 whole, which is shorter than its diff:
```python
import functools

import jax
import jax.numpy as jnp
from jax import lax
from jax.experimental import pallas as pl
from jax.experimental.pallas import tpu as pltpu
from jax.sharding import PartitionSpec as P

MESH = pl.DeviceIdType.MESH
alpha_res = 2.0**0.5
eps_norm = 1e-05
F32 = jnp.float32
BF16 = jnp.bfloat16


def dot32(a, b):
    return jnp.dot(a, b, preferred_element_type=F32)


def attention_kernel(
    chunk,
    tokens_hbm,
    state_hbm,
    wq_hbm,
    wk_hbm,
    wd_hbm,
    wv_hbm,
    wg_hbm,
    gain_hbm,
    new_hbm,
    gated_ref,
    tokens,
    state,
    fresh,
    wq,
    wk,
    wd,
    wv,
    wg,
    gain,
    readout,
    in_sem,
    state_sem,
    out_sem,
):
    rows, heads, key_dim, value_dim = state.shape
    chunks = rows // chunk
    small = [
        (tokens_hbm, tokens),
        (wk_hbm, wk),
        (wd_hbm, wd),
        (wq_hbm, wq),
        (wv_hbm, wv),
        (wg_hbm, wg),
        (gain_hbm, gain),
    ]
    copies = [
        pltpu.make_async_copy(src, dst, in_sem.at[n]) for n, (src, dst) in enumerate(small)
    ]
    ins = [
        pltpu.make_async_copy(
            state_hbm.at[pl.ds(n * chunk, chunk)], state.at[pl.ds(n * chunk, chunk)], state_sem.at[n]
        )
        for n in range(chunks)
    ]
    outs = [
        pltpu.make_async_copy(
            fresh.at[pl.ds(n * chunk, chunk)], new_hbm.at[pl.ds(n * chunk, chunk)], out_sem.at[n]
        )
        for n in range(chunks)
    ]
    for n in range(5):
        copies[n].start()
    for one in ins:
        one.start()
    copies[5].start()
    copies[6].start()

    copies[0].wait()
    x = tokens[...]
    copies[1].wait()
    keys = dot32(x, wk[...])
    copies[2].wait()
    pre = dot32(x, wd[...])
    decay = jnp.exp((jnp.minimum(pre, 0.0) - jnp.log1p(jnp.exp(-jnp.abs(pre)))) / 16.0)
    copies[3].wait()
    queries = dot32(x, wq[...]) * key_dim ** (-0.5)
    copies[4].wait()
    values = dot32(x, wv[...])
    columns = []
    for h in range(heads):
        part = slice(h * key_dim, (h + 1) * key_dim)
        pad = jnp.zeros((key_dim - 3 * rows, key_dim), F32)
        stacked = jnp.concatenate([keys[:, part], decay[:, part], queries[:, part], pad], axis=0)
        columns.append(stacked.T)
    for n in range(chunks):
        ins[n].wait()
        for b in range(n * chunk, (n + 1) * chunk):
            for h in range(heads):
                col = columns[h]
                v = values[b : b + 1, h * value_dim : (h + 1) * value_dim]
                new = (
                    col[:, rows + b : rows + b + 1] * state[b, h]
                    + col[:, b : b + 1] * v
                )
                fresh[b, h] = new
                readout[b : b + 1, h * value_dim : (h + 1) * value_dim] = jnp.sum(
                    col[:, 2 * rows + b : 2 * rows + b + 1] * new, axis=0, keepdims=True
                )
        outs[n].start()
    copies[5].wait()
    gate = dot32(x, wg[...])
    copies[6].wait()
    for h in range(heads):
        part = slice(h * value_dim, (h + 1) * value_dim)
        r = readout[:, part]
        scale = lax.rsqrt(jnp.mean(r * r, axis=-1, keepdims=True) + eps_norm)
        gated_ref[:, part] = (r * scale * gain[...] * jax.nn.silu(gate[:, part])).astype(BF16)
    for one in outs:
        one.wait()


def layer_kernel(
    n_ep,
    n_tp,
    group_count,
    cap,
    gated_hbm,
    wo_hbm,
    tokens_hbm,
    norm_gain_hbm,
    norm_bias_hbm,
    group_hbm,
    router_hbm,
    routes_hbm,
    eg_hbm,
    eu_hbm,
    ed_hbm,
    out_ref,
    gated,
    wo,
    tokens,
    norm_gain,
    norm_bias,
    group_w,
    router_w,
    routes,
    eg,
    eu,
    ed,
    part_mine,
    part_other,
    outgoing,
    arrived,
    results,
    returned,
    stat_mine,
    stat_other,
    in_sem,
    pair_sem,
    stat_sem,
    go_send,
    go_recv,
    back_send,
    back_recv,
):
    me = lax.axis_index("ep")
    core = lax.axis_index("tp")
    rows, width = tokens.shape
    half = width // n_tp
    experts = router_w.shape[1]
    per_group = experts // group_count
    slots = n_ep * cap
    pairs = [
        (gated_hbm, gated),
        (wo_hbm, wo),
        (tokens_hbm, tokens),
        (norm_gain_hbm, norm_gain),
        (norm_bias_hbm, norm_bias),
        (routes_hbm, routes),
        (group_hbm, group_w),
        (router_hbm, router_w),
        (eg_hbm, eg),
        (eu_hbm, eu),
        (ed_hbm, ed),
    ]
    loads = [
        pltpu.make_async_copy(src, dst, in_sem.at[n]) for n, (src, dst) in enumerate(pairs)
    ]
    barrier = pltpu.get_barrier_semaphore()
    for c in range(1, n_tp):
        pl.semaphore_signal(
            barrier, inc=1, device_id=(me, lax.rem(core + c, n_tp)), device_id_type=MESH
        )

    def greet(i, carry):
        there = lax.rem(me + i, n_ep)
        for c in range(n_tp):
            pl.semaphore_signal(barrier, inc=1, device_id=(there, c), device_id_type=MESH)
        return carry

    lax.fori_loop(1, n_ep, greet, 0)
    for one in loads:
        one.start()

    loads[0].wait()
    loads[1].wait()
    part_mine[...] = dot32(gated[...], wo[...]).astype(BF16)

    loads[5].wait()
    chosen = routes[...]
    first, second = chosen[:, 0:1], chosen[:, 1:2]
    below = (
        lax.broadcasted_iota(jnp.int32, (rows, rows), 1)
        < lax.broadcasted_iota(jnp.int32, (rows, rows), 0)
    ).astype(BF16)

    def slot_of(count, to_expert):
        column = lax.broadcasted_iota(jnp.int32, (rows, count), 1)
        expert = to_expert(lax.div(column, cap))
        place = lax.rem(column, cap).astype(F32)
        hit0, hit1 = first == expert, second == expert
        either = jnp.where(hit0, 1.0, jnp.where(hit1, 1.0, 0.0))
        earlier = dot32(below, either.astype(BF16))
        placed = jnp.where(earlier == place, 1.0, 0.0)
        return jnp.where(hit0, placed, 0.0), jnp.where(hit1, placed, 0.0)

    send0, send1 = slot_of(slots, lambda j: j * n_tp + core)
    pick_send = (send0 + send1).astype(BF16)
    back0, back1 = slot_of(slots * n_tp, lambda j: j)
    back0, back1 = back0.astype(BF16), back1.astype(BF16)

    pl.semaphore_wait(barrier, n_ep * n_tp - 1)
    swap = pltpu.make_async_remote_copy(
        src_ref=part_mine,
        dst_ref=part_other,
        send_sem=pair_sem.at[0],
        recv_sem=pair_sem.at[1],
        device_id=(me, 1 - core),
        device_id_type=MESH,
    )
    swap.start()
    for n in (2, 3, 4):
        loads[n].wait()
    base = alpha_res * tokens[...].astype(F32) + part_mine[...].astype(F32)
    swap.wait()
    mixed = base + part_other[...].astype(F32)
    centered = mixed - jnp.mean(mixed, axis=-1, keepdims=True)
    spread = jnp.mean(centered * centered, axis=-1, keepdims=True)
    hidden = (
        centered * lax.rsqrt(spread + eps_norm) * norm_gain[0:1, :] + norm_bias[0:1, :]
    ).astype(BF16)

    packed = lax.dot_general(
        pick_send, hidden, (((0,), (0,)), ((), ())), preferred_element_type=F32
    )
    outgoing[...] = packed.reshape(n_ep, cap, width).astype(BF16)

    def dispatch(i):
        there = lax.rem(me + i, n_ep)
        return pltpu.make_async_remote_copy(
            src_ref=outgoing.at[there],
            dst_ref=arrived.at[me],
            send_sem=go_send.at[i],
            recv_sem=go_recv.at[i],
            device_id=(there, core),
            device_id_type=MESH,
        )

    def go(i, carry):
        dispatch(i).start()
        return carry

    lax.fori_loop(1, n_ep, go, 0)
    arrived[me] = outgoing[me]

    loads[6].wait()
    loads[7].wait()
    group_logit = dot32(hidden, group_w[...])
    expert_logit = dot32(hidden, router_w[...])
    own_group = lax.div(first, per_group)
    group_hit = own_group == lax.broadcasted_iota(jnp.int32, group_logit.shape, 1)
    own_logit = jnp.sum(jnp.where(group_hit, group_logit, 0.0), axis=1, keepdims=True)
    share = 1.0 / jnp.sum(jnp.exp(group_logit - own_logit), axis=1, keepdims=True)
    expert_iota = lax.broadcasted_iota(jnp.int32, expert_logit.shape, 1)
    logit0 = jnp.sum(jnp.where(first == expert_iota, expert_logit, 0.0), axis=1, keepdims=True)
    logit1 = jnp.sum(jnp.where(second == expert_iota, expert_logit, 0.0), axis=1, keepdims=True)
    weight0 = share * jax.nn.sigmoid(logit0 - logit1)
    weight1 = share * jax.nn.sigmoid(logit1 - logit0)
    for n in (8, 9, 10):
        loads[n].wait()

    def landed(i, carry):
        dispatch(i).wait()
        return carry

    lax.fori_loop(1, n_ep, landed, 0)
    rows_in = arrived[...].astype(F32).reshape(slots, width).astype(BF16)
    gate_part = dot32(rows_in, eg[0])
    up_part = dot32(rows_in, eu[0])
    activation = (jax.nn.silu(gate_part) * up_part).astype(BF16)
    result = dot32(activation, ed[0]).reshape(n_ep, cap, width).astype(BF16)
    for c in range(n_tp):
        results[c] = result[:, :, c * half : (c + 1) * half]

    def send_back(i, c):
        there = lax.rem(me + i, n_ep)
        to = lax.rem(core + c, n_tp)
        return pltpu.make_async_remote_copy(
            src_ref=results.at[to, there],
            dst_ref=returned.at[me * n_tp + core],
            send_sem=back_send.at[c, i],
            recv_sem=back_recv.at[c, i],
            device_id=(there, to),
            device_id_type=MESH,
        )

    def back(i, carry):
        for c in range(n_tp):
            send_back(i, c).start()
        return carry

    lax.fori_loop(1, n_ep, back, 0)
    for c in range(1, n_tp):
        send_back(0, c).start()
    returned[me * n_tp + core] = results[core, me]
    mine = jnp.where(core == 0, hidden[:, :half].astype(F32), hidden[:, half:].astype(F32))
    base = alpha_res * mine
    gain = jnp.where(core == 0, norm_gain[1:2, :half], norm_gain[1:2, half:])
    shift = jnp.where(core == 0, norm_bias[1:2, :half], norm_bias[1:2, half:])

    def home(i, carry):
        for c in range(n_tp):
            send_back(i, c).wait()
        return carry

    lax.fori_loop(1, n_ep, home, 0)
    for c in range(1, n_tp):
        send_back(0, c).wait()
    fetched = returned[...].astype(F32).reshape(slots * n_tp, half).astype(BF16)
    blended = base + weight0 * dot32(back0, fetched) + weight1 * dot32(back1, fetched)
    total = jnp.sum(blended, axis=1, keepdims=True)
    squares = jnp.sum(blended * blended, axis=1, keepdims=True)
    lane = lax.broadcasted_iota(jnp.int32, stat_mine.shape, 1)
    stats = jnp.where(lane == 0, total, squares)
    stat_mine[...] = stats
    trade = pltpu.make_async_remote_copy(
        src_ref=stat_mine,
        dst_ref=stat_other,
        send_sem=stat_sem.at[0],
        recv_sem=stat_sem.at[1],
        device_id=(me, 1 - core),
        device_id_type=MESH,
    )
    trade.start()
    trade.wait()
    both = stats + stat_other[...]
    row_mean = both[:, 0:1] / width
    spread = both[:, 1:2] / width - row_mean * row_mean
    out_ref[...] = (
        (blended - row_mean) * lax.rsqrt(spread + eps_norm) * gain + shift
    ).astype(BF16)


def on_device(
    n_ep,
    n_tp,
    tokens,
    recurrent_state,
    query_weight,
    key_weight,
    decay_weight,
    value_weight,
    gate_weight,
    head_gain,
    output_weight,
    norm_gain,
    norm_bias,
    group_router,
    router_weight,
    routes,
    expert_gate,
    expert_up,
    expert_down,
):
    rows, width = tokens.shape
    heads, key_dim, value_dim = recurrent_state.shape[1:]
    anywhere = pl.BlockSpec(memory_space=pl.ANY)
    vmem = pl.BlockSpec(memory_space=pltpu.VMEM)
    chunk = 2
    chunks = rows // chunk
    dma = pltpu.SemaphoreType.DMA

    def like(a):
        return pltpu.VMEM(a.shape, a.dtype)

    gain_row = head_gain.reshape(1, value_dim)
    new_state, gated = pl.pallas_call(
        functools.partial(attention_kernel, chunk),
        out_shape=(
            jax.ShapeDtypeStruct(recurrent_state.shape, F32),
            jax.ShapeDtypeStruct((rows, heads * value_dim), BF16),
        ),
        in_specs=[anywhere] * 8,
        out_specs=(anywhere, vmem),
        scratch_shapes=[
            like(tokens),
            like(recurrent_state),
            like(recurrent_state),
            like(query_weight),
            like(key_weight),
            like(decay_weight),
            like(value_weight),
            like(gate_weight),
            like(gain_row),
            pltpu.VMEM((rows, heads * value_dim), F32),
            dma((7,)),
            dma((chunks,)),
            dma((chunks,)),
        ],
        compiler_params=pltpu.CompilerParams(vmem_limit_bytes=40 * 1024 * 1024),
        name="attention",
    )(
        tokens,
        recurrent_state,
        query_weight,
        key_weight,
        decay_weight,
        value_weight,
        gate_weight,
        gain_row,
    )
    experts = router_weight.shape[1]
    cap = 2 * max(1, rows // experts)
    half = width // n_tp
    operands = (
        gated,
        output_weight,
        tokens,
        norm_gain,
        norm_bias,
        group_router,
        router_weight,
        routes,
        expert_gate,
        expert_up,
        expert_down,
    )
    new_tokens = pl.pallas_call(
        functools.partial(layer_kernel, n_ep, n_tp, group_router.shape[1], cap),
        out_shape=jax.ShapeDtypeStruct((rows, half), BF16),
        in_specs=[anywhere] * len(operands),
        out_specs=vmem,
        scratch_shapes=[like(a) for a in operands]
        + [
            pltpu.VMEM((rows, width), BF16),
            pltpu.VMEM((rows, width), BF16),
            pltpu.VMEM((n_ep, cap, width), BF16),
            pltpu.VMEM((n_ep, cap, width), BF16),
            pltpu.VMEM((n_tp, n_ep, cap, half), BF16),
            pltpu.VMEM((n_ep * n_tp, cap, half), BF16),
            pltpu.VMEM((rows, 128), F32),
            pltpu.VMEM((rows, 128), F32),
            dma((len(operands),)),
            dma((2,)),
            dma((2,)),
            dma((n_ep,)),
            dma((n_ep,)),
            dma((n_tp, n_ep)),
            dma((n_tp, n_ep)),
        ],
        compiler_params=pltpu.CompilerParams(
            collective_id=0, has_side_effects=True, vmem_limit_bytes=40 * 1024 * 1024
        ),
        name="layer",
    )(*operands)
    return new_tokens, new_state


def solution(mesh):
    in_specs = (
        P("ep", None),
        P("ep", "tp", None, None),
        P(None, "tp"),
        P(None, "tp"),
        P(None, "tp"),
        P(None, "tp"),
        P(None, "tp"),
        P(),
        P("tp", None),
        P(),
        P(),
        P(),
        P(),
        P("ep", None),
        P(("ep", "tp"), None, None),
        P(("ep", "tp"), None, None),
        P(("ep", "tp"), None, None),
    )
    out_specs = (P("ep", "tp"), P("ep", "tp", None, None))
    return jax.shard_map(
        functools.partial(on_device, mesh.shape["ep"], mesh.shape["tp"]),
        mesh=mesh,
        in_specs=in_specs,
        out_specs=out_specs,
        check_vma=False,
    )
```

time: 94.9 us -> 43.2 us (0.46)
  waiting for transfers between devices: 31.1 us -> 0 us
  Pallas kernels: 0 us -> 27.8 us
  between operations: 14.4 us -> 0.74 us
  matrix products: 13.3 us -> 0 us
  other arithmetic: 12.1 us -> 0 us
  starting transfers between devices: 10.4 us -> 0 us
  local copies, waits for them, and re-layouts: 6.53 us -> 14.2 us
  blocking collectives: 6.31 us -> 0 us
    pallas_call x0 -> x2, Pallas kernels: none -> 27.8 us  [the longest x1 22.1 us: on_device(): pl.pallas_call(functools.partial(layer_kernel, n_ep, n_tp, group_router.s...]
    psum x1 -> x0, waiting for transfers between devices: 16.7 us -> none  [on_device(): lax.psum(partial_value.astype(jnp.bfloat16), 'tp').astype(jnp.float32)]
    all_to_all x2 -> x0, waiting for transfers between devices: 14.4 us -> none  [the longest x1 7.57 us: on_device(): lax.all_to_all(results, 'ep', split_axis=0, concat_axis=0, tiled=True)]
    dot_general x11 -> x0, matrix products: 13.3 us -> none  [the longest x4 5.4 us: project(): return jnp.dot(tokens, weight, preferred_element_type=jnp.float32)]
    unnamed x26 -> x32, local copies, waits for them, and re-layouts: 1.93 us -> 14.2 us
    all_to_all x2 -> x0, starting transfers between devices: 10.3 us -> none  [the longest x1 6.83 us: on_device(): lax.all_to_all(outgoing, 'ep', split_axis=0, concat_axis=0, tiled=True)]
    reduce_sum x9 -> x0, other arithmetic: 8.28 us -> none  [the longest x1 5.65 us: on_device(): readout = jnp.sum(queries[..., None] * new_state, axis=2)]
    all_to_all x1 -> x0, blocking collectives: 3.84 us -> none  [on_device(): lax.all_to_all(lax.all_to_all(results, 'ep', split_axis=0, concat_axis=0,...]
  transfers between devices with their start and end apart: 3 -> 0, of which waited for: 3 -> 0; matrix products, arithmetic and copies ran while one was open for 5% -> 0% of each run, Pallas kernels for 0% -> 0%
where the time goes in v1:
time: 43.2 us; the launch traced here: 42.7 us
  Pallas kernels  27.8 us (64%)
  local copies, waits for them, and re-layouts  14.2 us (33%)
  between operations  0.74 us (2%)
    pallas_call x1, Pallas kernels, on_device(): pl.pallas_call(functools.partial(layer_kernel, n_ep, n_tp, group_router.s...  22.1 us
    unnamed x32, local copies, waits for them, and re-layouts  14.2 us
    pallas_call x1, Pallas kernels, on_device(): pl.pallas_call(functools.partial(attention_kernel, chunk), out_shape=(jax...  5.69 us

profile of v1, /device:TPU:0, one launch (start us, length us, event | category | flops | bytes accessed | tf_op | source)
XLA Modules:
  0.0 42.7 jit_solution(9543758017743101481)
XLA Ops:
  0.6 0.8 %copy.21.routes_hbm = s32[16,2]{1,0:T(8,128)S(1)} copy(s32[16,2]{0,1:T(2,128)} %param.30) | data formatting | bytes 256 | tf_op args[13]
  1.4 1.0 %copy.19.group_hbm = bf16[2048,4]{1,0:T(8,128)(2,1)S(1)} copy(bf16[2048,4]{0,1:T(4,128)(2,1)} %param.28) | data formatting | bytes 32768 | tf_op args[11]
  2.4 1.2 %copy.20.router_hbm = bf16[2048,32]{1,0:T(8,128)(2,1)S(1)} copy(bf16[2048,32]{0,1:T(8,128)(2,1)} %param.29) | data formatting | bytes 262144 | tf_op args[12]
  3.6 0.0 copy-start
  3.6 2.2 %copy-done = f32[16,2,128,256]{3,2,1,0:T(8,128)S(1)} copy-done((f32[16,2,128,256]{3,2,1,0:T(8,128)S(1)}, f32[16,2,128,256]{3,2,1,0:T(8,128)}, u32[]{:S(2)}) %copy-start) | copy-done | bytes 4194328
  5.8 0.0 copy-start.2
  5.8 1.6 %copy-done.2 = bf16[2048,512]{1,0:T(8,128)(2,1)S(1)} copy-done((bf16[2048,512]{1,0:T(8,128)(2,1)S(1)}, bf16[2048,512]{1,0:T(8,128)(2,1)}, u32[]{:S(2)}) %copy-start.2) | copy-done | bytes 2097176
  7.4 0.0 copy-start.3
  7.4 1.6 %copy-done.3 = bf16[2048,512]{1,0:T(8,128)(2,1)S(1)} copy-done((bf16[2048,512]{1,0:T(8,128)(2,1)S(1)}, bf16[2048,512]{1,0:T(8,128)(2,1)}, u32[]{:S(2)}) %copy-start.3) | copy-done | bytes 2097176
  9.0 0.0 copy-start.4
  9.0 1.2 %copy-done.4 = bf16[2048,256]{1,0:T(8,128)(2,1)S(1)} copy-done((bf16[2048,256]{1,0:T(8,128)(2,1)S(1)}, bf16[2048,256]{1,0:T(8,128)(2,1)}, u32[]{:S(2)}) %copy-start.4) | copy-done | bytes 1048600
  10.2 0.0 copy-start.5
  10.2 1.2 %copy-done.5 = bf16[2048,256]{1,0:T(8,128)(2,1)S(1)} copy-done((bf16[2048,256]{1,0:T(8,128)(2,1)S(1)}, bf16[2048,256]{1,0:T(8,128)(2,1)}, u32[]{:S(2)}) %copy-start.5) | copy-done | bytes 1048600
  11.4 0.0 copy-start.6
  11.4 1.2 %copy-done.6 = bf16[2048,256]{1,0:T(8,128)(2,1)S(1)} copy-done((bf16[2048,256]{1,0:T(8,128)(2,1)S(1)}, bf16[2048,256]{1,0:T(8,128)(2,1)}, u32[]{:S(2)}) %copy-start.6) | copy-done | bytes 1048600
  12.7 0.8 %copy-done.10 = bf16[16,2048]{1,0:T(8,128)(2,1)S(1)} copy-done((bf16[16,2048]{1,0:T(8,128)(2,1)S(1)}, bf16[16,2048]{1,0:T(8,128)(2,1)}, u32[]{:S(2)}) %copy-start.10) | copy-done | bytes 65560
  13.5 0.7 %copy-done.13 = f32[256]{0:T(256)S(1)} copy-done((f32[256]{0:T(256)S(1)}, f32[256]{0:T(256)}, u32[]{:S(2)}) %copy-start.13) | copy-done | bytes 1048
  14.2 0.0 copy-start.1
  14.2 0.0 copy-start.7
  14.2 0.0 copy-start.8
  14.2 0.0 copy-start.9
  14.2 0.0 copy-start.11
  14.2 0.0 copy-start.12
  14.2 5.7 %attention.1 = (f32[16,2,128,256]{3,2,1,0:T(8,128)}, bf16[16,512]{1,0:T(8,128)(2,1)S(1)}) custom-call(bf16[16,2048]{1,0:T(8,128)(2,1)S(1)} %copy-done.10, f32[16,2,128,256]{3,2,1,0:T(8,128)S(1)} %copy-done, bf16[2048,256]{1,0:T(8,128)(2,1)S(1)} %copy-done.4, bf16[2048,256]{1,0:T(8,128)(2,1)S(1)} %copy-done.5, bf16[2048,256]{1,0:T(8,128)(2,1)S(1)} %copy-done.6, ...), custom_call_target="tpu_custom_call" | custom-call | tf_op jit(solution)/shard_map/attention/pallas_call | solution.py:399
  19.9 0.0 copy-done.1
  19.9 0.0 copy-done.7
  19.9 0.0 copy-done.8
  19.9 0.0 copy-done.9
  20.0 0.0 copy-done.11
  20.0 0.0 copy-done.12
  20.0 22.1 %layer.1 = bf16[16,1024]{1,0:T(8,128)(2,1)S(1)} custom-call(bf16[16,512]{1,0:T(8,128)(2,1)S(1)} %get-tuple-element.4.gated_hbm, bf16[512,2048]{1,0:T(8,128)(2,1)S(1)} %copy-done.1, bf16[16,2048]{1,0:T(8,128)(2,1)S(1)} %copy-done.10, f32[2,2048]{1,0:T(2,128)S(1)} %copy-done.11, f32[2,2048]{1,0:T(2,128)S(1)} %copy-done.12, ...), custom_call_target="tpu_custom_call" | custom-call | tf_op jit(solution)/shard_map/layer/pallas_call | solution.py:450
  42.1 0.6 %copy.23 = bf16[16,1024]{1,0:T(8,128)(2,1)} copy(bf16[16,1024]{1,0:T(8,128)(2,1)S(1)} %layer.1) | data formatting | bytes 65536
  (2 shorter events, 0.0 us)
Async XLA Ops:
  3.6 2.2 %copy-start = (f32[16,2,128,256]{3,2,1,0:T(8,128)S(1)}, f32[16,2,128,256]{3,2,1,0:T(8,128)}, u32[]{:S(2)}) copy-start(f32[16,2,128,256]{3,2,1,0:T(8,128)} %state_hbm.1) | copy-start | bytes 12582916
  5.8 1.6 %copy-start.2 = (bf16[2048,512]{1,0:T(8,128)(2,1)S(1)}, bf16[2048,512]{1,0:T(8,128)(2,1)}, u32[]{:S(2)}) copy-start(bf16[2048,512]{1,0:T(8,128)(2,1)} %wv_hbm.1) | copy-start | bytes 6291460
  7.4 1.6 %copy-start.3 = (bf16[2048,512]{1,0:T(8,128)(2,1)S(1)}, bf16[2048,512]{1,0:T(8,128)(2,1)}, u32[]{:S(2)}) copy-start(bf16[2048,512]{1,0:T(8,128)(2,1)} %wg_hbm.1) | copy-start | bytes 6291460
  9.0 1.2 %copy-start.4 = (bf16[2048,256]{1,0:T(8,128)(2,1)S(1)}, bf16[2048,256]{1,0:T(8,128)(2,1)}, u32[]{:S(2)}) copy-start(bf16[2048,256]{1,0:T(8,128)(2,1)} %wq_hbm.1) | copy-start | bytes 3145732
  10.2 1.2 %copy-start.5 = (bf16[2048,256]{1,0:T(8,128)(2,1)S(1)}, bf16[2048,256]{1,0:T(8,128)(2,1)}, u32[]{:S(2)}) copy-start(bf16[2048,256]{1,0:T(8,128)(2,1)} %wk_hbm.1) | copy-start | bytes 3145732
  11.4 1.2 %copy-start.6 = (bf16[2048,256]{1,0:T(8,128)(2,1)S(1)}, bf16[2048,256]{1,0:T(8,128)(2,1)}, u32[]{:S(2)}) copy-start(bf16[2048,256]{1,0:T(8,128)(2,1)} %wd_hbm.1) | copy-start | bytes 3145732
  12.7 0.8 %copy-start.10 = (bf16[16,2048]{1,0:T(8,128)(2,1)S(1)}, bf16[16,2048]{1,0:T(8,128)(2,1)}, u32[]{:S(2)}) copy-start(bf16[16,2048]{1,0:T(8,128)(2,1)} %tokens_hbm.3) | copy-start | bytes 196612
  13.5 0.7 %copy-start.13 = (f32[256]{0:T(256)S(1)}, f32[256]{0:T(256)}, u32[]{:S(2)}) copy-start(f32[256]{0:T(256)} %param.24) | copy-start | bytes 3076
  14.2 5.7 %copy-start.1 = (bf16[512,2048]{1,0:T(8,128)(2,1)S(1)}, bf16[512,2048]{1,0:T(8,128)(2,1)}, u32[]{:S(2)}) copy-start(bf16[512,2048]{1,0:T(8,128)(2,1)} %wo_hbm.1) | copy-start | bytes 6291460
  14.2 5.7 %copy-start.7 = (bf16[1,2048,256]{2,1,0:T(8,128)(2,1)S(1)}, bf16[1,2048,256]{2,1,0:T(8,128)(2,1)}, u32[]{:S(2)}) copy-start(bf16[1,2048,256]{2,1,0:T(8,128)(2,1)} %eg_hbm.1) | copy-start | bytes 3145732
  14.2 5.8 %copy-start.8 = (bf16[1,2048,256]{2,1,0:T(8,128)(2,1)S(1)}, bf16[1,2048,256]{2,1,0:T(8,128)(2,1)}, u32[]{:S(2)}) copy-start(bf16[1,2048,256]{2,1,0:T(8,128)(2,1)} %eu_hbm.1) | copy-start | bytes 3145732
  14.2 5.8 %copy-start.9 = (bf16[1,256,2048]{2,1,0:T(8,128)(2,1)S(1)}, bf16[1,256,2048]{2,1,0:T(8,128)(2,1)}, u32[]{:S(2)}) copy-start(bf16[1,256,2048]{2,1,0:T(8,128)(2,1)} %ed_hbm.1) | copy-start | bytes 3145732
  14.2 5.8 %copy-start.11 = (f32[2,2048]{1,0:T(2,128)S(1)}, f32[2,2048]{1,0:T(2,128)}, u32[]{:S(2)}) copy-start(f32[2,2048]{1,0:T(2,128)} %norm_gain_hbm.1) | copy-start | bytes 49156
  14.2 5.8 %copy-start.12 = (f32[2,2048]{1,0:T(2,128)S(1)}, f32[2,2048]{1,0:T(2,128)}, u32[]{:S(2)}) copy-start(f32[2,2048]{1,0:T(2,128)} %norm_bias_hbm.1) | copy-start | bytes 49156

commit v2 on v1

--- a/solution.py
+++ b/solution.py
@@ -29,7 +29,7 @@
     wg_hbm,
     gain_hbm,
     new_hbm,
-    gated_ref,
+    gated_hbm,
     tokens,
     state,
     fresh,
@@ -40,9 +40,11 @@
     wg,
     gain,
     readout,
+    gated_ref,
     in_sem,
     state_sem,
     out_sem,
+    gated_sem,
 ):
     rows, heads, key_dim, value_dim = state.shape
     chunks = rows // chunk
@@ -117,22 +119,24 @@
         r = readout[:, part]
         scale = lax.rsqrt(jnp.mean(r * r, axis=-1, keepdims=True) + eps_norm)
         gated_ref[:, part] = (r * scale * gain[...] * jax.nn.silu(gate[:, part])).astype(BF16)
+    rounded = pltpu.make_async_copy(gated_ref, gated_hbm, gated_sem.at[0])
+    rounded.start()
     for one in outs:
         one.wait()
+    rounded.wait()
 
 
 def layer_kernel(
     n_ep,
     n_tp,
-    group_count,
     cap,
     gated_hbm,
     wo_hbm,
     tokens_hbm,
     norm_gain_hbm,
     norm_bias_hbm,
-    group_hbm,
-    router_hbm,
+    group_w_hbm,
+    router_w_hbm,
     routes_hbm,
     eg_hbm,
     eu_hbm,
@@ -169,67 +173,81 @@
     core = lax.axis_index("tp")
     rows, width = tokens.shape
     half = width // n_tp
-    experts = router_w.shape[1]
-    per_group = experts // group_count
+    per_group = router_w.shape[0] // group_w.shape[0]
     slots = n_ep * cap
-    pairs = [
+    operands = [
         (gated_hbm, gated),
         (wo_hbm, wo),
+        (routes_hbm, routes),
         (tokens_hbm, tokens),
         (norm_gain_hbm, norm_gain),
         (norm_bias_hbm, norm_bias),
-        (routes_hbm, routes),
-        (group_hbm, group_w),
-        (router_hbm, router_w),
+        (group_w_hbm, group_w),
+        (router_w_hbm, router_w),
         (eg_hbm, eg),
         (eu_hbm, eu),
         (ed_hbm, ed),
     ]
+    order = sorted(range(1, n_ep), key=lambda i: abs(2 * i - n_ep))
+
+    def over_peers(body):
+        if n_ep <= 32:
+            for i in order:
+                body(i)
+        else:
+
+            def step(i, carry):
+                body(i)
+                return carry
+
+            lax.fori_loop(1, n_ep, step, 0)
+
+    barrier = pltpu.get_barrier_semaphore()
+
+    def greet(i):
+        for c in range(n_tp):
+            pl.semaphore_signal(
+                barrier, inc=1, device_id=(lax.rem(me + i, n_ep), c), device_id_type=MESH
+            )
+
     loads = [
-        pltpu.make_async_copy(src, dst, in_sem.at[n]) for n, (src, dst) in enumerate(pairs)
+        pltpu.make_async_copy(src, dst, in_sem.at[n]) for n, (src, dst) in enumerate(operands)
     ]
-    barrier = pltpu.get_barrier_semaphore()
+    for one in loads:
+        one.start()
+    over_peers(greet)
     for c in range(1, n_tp):
         pl.semaphore_signal(
             barrier, inc=1, device_id=(me, lax.rem(core + c, n_tp)), device_id_type=MESH
         )
 
-    def greet(i, carry):
-        there = lax.rem(me + i, n_ep)
-        for c in range(n_tp):
-            pl.semaphore_signal(barrier, inc=1, device_id=(there, c), device_id_type=MESH)
-        return carry
-
-    lax.fori_loop(1, n_ep, greet, 0)
-    for one in loads:
-        one.start()
-
     loads[0].wait()
     loads[1].wait()
     part_mine[...] = dot32(gated[...], wo[...]).astype(BF16)
 
-    loads[5].wait()
-    chosen = routes[...]
-    first, second = chosen[:, 0:1], chosen[:, 1:2]
-    below = (
-        lax.broadcasted_iota(jnp.int32, (rows, rows), 1)
-        < lax.broadcasted_iota(jnp.int32, (rows, rows), 0)
+    loads[2].wait()
+    first, second = routes[0:1, :], routes[1:2, :]
+    before = (
+        lax.broadcasted_iota(jnp.int32, (rows, rows), 0)
+        < lax.broadcasted_iota(jnp.int32, (rows, rows), 1)
     ).astype(BF16)
 
     def slot_of(count, to_expert):
-        column = lax.broadcasted_iota(jnp.int32, (rows, count), 1)
-        expert = to_expert(lax.div(column, cap))
-        place = lax.rem(column, cap).astype(F32)
+        line = lax.broadcasted_iota(jnp.int32, (count, rows), 0)
+        expert = to_expert(lax.div(line, cap))
+        place = lax.rem(line, cap).astype(F32)
         hit0, hit1 = first == expert, second == expert
         either = jnp.where(hit0, 1.0, jnp.where(hit1, 1.0, 0.0))
-        earlier = dot32(below, either.astype(BF16))
+        earlier = dot32(either.astype(BF16), before)
         placed = jnp.where(earlier == place, 1.0, 0.0)
         return jnp.where(hit0, placed, 0.0), jnp.where(hit1, placed, 0.0)
 
     send0, send1 = slot_of(slots, lambda j: j * n_tp + core)
     pick_send = (send0 + send1).astype(BF16)
     back0, back1 = slot_of(slots * n_tp, lambda j: j)
-    back0, back1 = back0.astype(BF16), back1.astype(BF16)
+    for n in range(3, len(loads)):
+        loads[n].wait()
+    base = alpha_res * tokens[...].astype(F32) + part_mine[...].astype(F32)
 
     pl.semaphore_wait(barrier, n_ep * n_tp - 1)
     swap = pltpu.make_async_remote_copy(
@@ -241,9 +259,6 @@
         device_id_type=MESH,
     )
     swap.start()
-    for n in (2, 3, 4):
-        loads[n].wait()
-    base = alpha_res * tokens[...].astype(F32) + part_mine[...].astype(F32)
     swap.wait()
     mixed = base + part_other[...].astype(F32)
     centered = mixed - jnp.mean(mixed, axis=-1, keepdims=True)
@@ -252,10 +267,7 @@
         centered * lax.rsqrt(spread + eps_norm) * norm_gain[0:1, :] + norm_bias[0:1, :]
     ).astype(BF16)
 
-    packed = lax.dot_general(
-        pick_send, hidden, (((0,), (0,)), ((), ())), preferred_element_type=F32
-    )
-    outgoing[...] = packed.reshape(n_ep, cap, width).astype(BF16)
+    outgoing[...] = dot32(pick_send, hidden).reshape(n_ep, cap, width).astype(BF16)
 
     def dispatch(i):
         there = lax.rem(me + i, n_ep)
@@ -268,47 +280,40 @@
             device_id_type=MESH,
         )
 
-    def go(i, carry):
-        dispatch(i).start()
-        return carry
-
-    lax.fori_loop(1, n_ep, go, 0)
+    over_peers(lambda i: dispatch(i).start())
     arrived[me] = outgoing[me]
 
-    loads[6].wait()
-    loads[7].wait()
-    group_logit = dot32(hidden, group_w[...])
-    expert_logit = dot32(hidden, router_w[...])
+    across = (((1,), (1,)), ((), ()))
+    group_logit = lax.dot_general(group_w[...], hidden, across, preferred_element_type=F32)
+    expert_logit = lax.dot_general(router_w[...], hidden, across, preferred_element_type=F32)
     own_group = lax.div(first, per_group)
-    group_hit = own_group == lax.broadcasted_iota(jnp.int32, group_logit.shape, 1)
-    own_logit = jnp.sum(jnp.where(group_hit, group_logit, 0.0), axis=1, keepdims=True)
-    share = 1.0 / jnp.sum(jnp.exp(group_logit - own_logit), axis=1, keepdims=True)
-    expert_iota = lax.broadcasted_iota(jnp.int32, expert_logit.shape, 1)
-    logit0 = jnp.sum(jnp.where(first == expert_iota, expert_logit, 0.0), axis=1, keepdims=True)
-    logit1 = jnp.sum(jnp.where(second == expert_iota, expert_logit, 0.0), axis=1, keepdims=True)
-    weight0 = share * jax.nn.sigmoid(logit0 - logit1)
-    weight1 = share * jax.nn.sigmoid(logit1 - logit0)
-    for n in (8, 9, 10):
-        loads[n].wait()
-
-    def landed(i, carry):
-        dispatch(i).wait()
-        return carry
-
-    lax.fori_loop(1, n_ep, landed, 0)
+    group_hit = own_group == lax.broadcasted_iota(jnp.int32, group_logit.shape, 0)
+    own_logit = jnp.sum(jnp.where(group_hit, group_logit, 0.0), axis=0, keepdims=True)
+    share = 1.0 / jnp.sum(jnp.exp(group_logit - own_logit), axis=0, keepdims=True)
+    expert_iota = lax.broadcasted_iota(jnp.int32, expert_logit.shape, 0)
+    logit0 = jnp.sum(jnp.where(first == expert_iota, expert_logit, 0.0), axis=0, keepdims=True)
+    logit1 = jnp.sum(jnp.where(second == expert_iota, expert_logit, 0.0), axis=0, keepdims=True)
+    weighted = back0 * (share * jax.nn.sigmoid(logit0 - logit1)) + back1 * (
+        share * jax.nn.sigmoid(logit1 - logit0)
+    )
+    upper = weighted.astype(BF16)
+    lower = (weighted - upper.astype(F32)).astype(BF16)
+    mine = jnp.where(core == 0, hidden[:, :half].astype(F32), hidden[:, half:].astype(F32))
+    base = alpha_res * mine
+    gain = jnp.where(core == 0, norm_gain[1:2, :half], norm_gain[1:2, half:])
+    shift = jnp.where(core == 0, norm_bias[1:2, :half], norm_bias[1:2, half:])
+
+    over_peers(lambda i: dispatch(i).wait())
     rows_in = arrived[...].astype(F32).reshape(slots, width).astype(BF16)
     gate_part = dot32(rows_in, eg[0])
     up_part = dot32(rows_in, eu[0])
     activation = (jax.nn.silu(gate_part) * up_part).astype(BF16)
-    result = dot32(activation, ed[0]).reshape(n_ep, cap, width).astype(BF16)
-    for c in range(n_tp):
-        results[c] = result[:, :, c * half : (c + 1) * half]
 
     def send_back(i, c):
         there = lax.rem(me + i, n_ep)
         to = lax.rem(core + c, n_tp)
         return pltpu.make_async_remote_copy(
-            src_ref=results.at[to, there],
+            src_ref=results.at[c, there],
             dst_ref=returned.at[me * n_tp + core],
             send_sem=back_send.at[c, i],
             recv_sem=back_recv.at[c, i],
@@ -316,30 +321,29 @@
             device_id_type=MESH,
         )
 
-    def back(i, carry):
-        for c in range(n_tp):
-            send_back(i, c).start()
-        return carry
-
-    lax.fori_loop(1, n_ep, back, 0)
-    for c in range(1, n_tp):
-        send_back(0, c).start()
-    returned[me * n_tp + core] = results[core, me]
-    mine = jnp.where(core == 0, hidden[:, :half].astype(F32), hidden[:, half:].astype(F32))
-    base = alpha_res * mine
-    gain = jnp.where(core == 0, norm_gain[1:2, :half], norm_gain[1:2, half:])
-    shift = jnp.where(core == 0, norm_bias[1:2, :half], norm_bias[1:2, half:])
-
-    def home(i, carry):
+    for c in range(n_tp):
+        start = pl.multiple_of(lax.rem(core + c, n_tp) * half, half)
+        result = dot32(activation, ed[0, :, pl.ds(start, half)])
+        results[c] = result.reshape(n_ep, cap, half).astype(BF16)
+        over_peers(lambda i: send_back(i, c).start())
+        if c:
+            send_back(0, c).start()
+    returned[me * n_tp + core] = results[0, me]
+
+    def home(i):
         for c in range(n_tp):
             send_back(i, c).wait()
-        return carry
-
-    lax.fori_loop(1, n_ep, home, 0)
+
+    over_peers(home)
     for c in range(1, n_tp):
         send_back(0, c).wait()
     fetched = returned[...].astype(F32).reshape(slots * n_tp, half).astype(BF16)
-    blended = base + weight0 * dot32(back0, fetched) + weight1 * dot32(back1, fetched)
+    down = (((0,), (0,)), ((), ()))
+    blended = (
+        base
+        + lax.dot_general(upper, fetched, down, preferred_element_type=F32)
+        + lax.dot_general(lower, fetched, down, preferred_element_type=F32)
+    )
     total = jnp.sum(blended, axis=1, keepdims=True)
     squares = jnp.sum(blended * blended, axis=1, keepdims=True)
     lane = lax.broadcasted_iota(jnp.int32, stat_mine.shape, 1)
@@ -386,7 +390,7 @@
 ):
     rows, width = tokens.shape
     heads, key_dim, value_dim = recurrent_state.shape[1:]
-    anywhere = pl.BlockSpec(memory_space=pl.ANY)
+    in_hbm = pl.BlockSpec(memory_space=pltpu.HBM)
     vmem = pl.BlockSpec(memory_space=pltpu.VMEM)
     chunk = 2
     chunks = rows // chunk
@@ -402,8 +406,8 @@
             jax.ShapeDtypeStruct(recurrent_state.shape, F32),
             jax.ShapeDtypeStruct((rows, heads * value_dim), BF16),
         ),
-        in_specs=[anywhere] * 8,
-        out_specs=(anywhere, vmem),
+        in_specs=[in_hbm] * 8,
+        out_specs=(in_hbm, in_hbm),
         scratch_shapes=[
             like(tokens),
             like(recurrent_state),
@@ -415,11 +419,13 @@
             like(gate_weight),
             like(gain_row),
             pltpu.VMEM((rows, heads * value_dim), F32),
+            pltpu.VMEM((rows, heads * value_dim), BF16),
             dma((7,)),
             dma((chunks,)),
             dma((chunks,)),
+            dma((1,)),
         ],
-        compiler_params=pltpu.CompilerParams(vmem_limit_bytes=40 * 1024 * 1024),
+        compiler_params=pltpu.CompilerParams(vmem_limit_bytes=67043328),
         name="attention",
     )(
         tokens,
@@ -440,17 +446,17 @@
         tokens,
         norm_gain,
         norm_bias,
-        group_router,
-        router_weight,
-        routes,
+        group_router.T,
+        router_weight.T,
+        routes.T,
         expert_gate,
         expert_up,
         expert_down,
     )
     new_tokens = pl.pallas_call(
-        functools.partial(layer_kernel, n_ep, n_tp, group_router.shape[1], cap),
+        functools.partial(layer_kernel, n_ep, n_tp, cap),
         out_shape=jax.ShapeDtypeStruct((rows, half), BF16),
-        in_specs=[anywhere] * len(operands),
+        in_specs=[in_hbm] * len(operands),
         out_specs=vmem,
         scratch_shapes=[like(a) for a in operands]
         + [
@@ -471,7 +477,7 @@
             dma((n_tp, n_ep)),
         ],
         compiler_params=pltpu.CompilerParams(
-            collective_id=0, has_side_effects=True, vmem_limit_bytes=40 * 1024 * 1024
+            collective_id=0, has_side_effects=True, vmem_limit_bytes=67043328
         ),
         name="layer",
     )(*operands)

time: 43.2 us -> 33 us (0.76)
  local copies, waits for them, and re-layouts: 14.2 us -> 1.38 us
  Pallas kernels: 27.8 us -> 30.7 us
    unnamed x32 -> x1, local copies, waits for them, and re-layouts: 14.2 us -> 1.38 us
    pallas_call x1, Pallas kernels: 5.69 us -> 7.45 us  [on_device(): pl.pallas_call(functools.partial(attention_kernel, chunk), out_shape=(jax...]
    pallas_call x1, Pallas kernels: 22.1 us -> 23.2 us  [on_device(): pl.pallas_call(functools.partial(layer_kernel, n_ep, n_tp, cap), out_shap...]
where the time goes in v2:
time: 33 us; the launch traced here: 32.7 us
  Pallas kernels  30.7 us (93%)
  local copies, waits for them, and re-layouts  1.38 us (4%)
  between operations  0.65 us (2%)
    pallas_call x1, Pallas kernels, on_device(): pl.pallas_call(functools.partial(layer_kernel, n_ep, n_tp, cap), out_shap...  23.2 us
    pallas_call x1, Pallas kernels, on_device(): pl.pallas_call(functools.partial(attention_kernel, chunk), out_shape=(jax...  7.45 us
    unnamed x1, local copies, waits for them, and re-layouts  1.38 us

profile of v2, /device:TPU:0, one launch (start us, length us, event | category | flops | bytes accessed | tf_op | source)
XLA Modules:
  0.0 32.7 jit_solution(8984703179212573902)
XLA Ops:
  0.6 7.5 %attention.1 = (f32[16,2,128,256]{3,2,1,0:T(8,128)}, bf16[16,512]{1,0:T(8,128)(2,1)}) custom-call(bf16[16,2048]{1,0:T(8,128)(2,1)} %tokens_hbm.3, f32[16,2,128,256]{3,2,1,0:T(8,128)} %state_hbm.1, bf16[2048,256]{1,0:T(8,128)(2,1)} %wq_hbm.1, bf16[2048,256]{1,0:T(8,128)(2,1)} %wk_hbm.1, bf16[2048,256]{1,0:T(8,128)(2,1)} %wd_hbm.1, bf16[2048,512]{1,0:T(8,128)(2,1)} %wv_hbm.1, ...), custom_call_target="tpu_custom_call" | custom-call | tf_op jit(solution)/shard_map/attention/pallas_call | solution.py:403
  8.1 23.2 %layer.1 = bf16[16,1024]{1,0:T(8,128)(2,1)} custom-call(bf16[16,512]{1,0:T(8,128)(2,1)} %get-tuple-element.4.gated_hbm, bf16[512,2048]{1,0:T(8,128)(2,1)} %wo_hbm.1, bf16[16,2048]{1,0:T(8,128)(2,1)} %tokens_hbm.3, f32[2,2048]{1,0:T(2,128)} %norm_gain_hbm.1, f32[2,2048]{1,0:T(2,128)} %norm_bias_hbm.1, bf16[4,2048]{1,0:T(4,128)(2,1)} %bitcast.5, ...), custom_call_target="tpu_custom_call" | custom-call | tf_op jit(solution)/shard_map/layer/pallas_call | solution.py:456
  31.3 1.4 %copy.20 = bf16[16,1024]{1,0:T(8,128)(2,1)} copy(bf16[16,1024]{1,0:T(8,128)(2,1)} %layer.1) | data formatting | bytes 65536

commit v3 on v2

--- a/solution.py
+++ b/solution.py
@@ -26,10 +26,9 @@
     wk_hbm,
     wd_hbm,
     wv_hbm,
-    wg_hbm,
     gain_hbm,
     new_hbm,
-    gated_hbm,
+    normed_hbm,
     tokens,
     state,
     fresh,
@@ -37,14 +36,13 @@
     wk,
     wd,
     wv,
-    wg,
     gain,
     readout,
-    gated_ref,
+    normed,
     in_sem,
     state_sem,
     out_sem,
-    gated_sem,
+    normed_sem,
 ):
     rows, heads, key_dim, value_dim = state.shape
     chunks = rows // chunk
@@ -54,7 +52,6 @@
         (wd_hbm, wd),
         (wq_hbm, wq),
         (wv_hbm, wv),
-        (wg_hbm, wg),
         (gain_hbm, gain),
     ]
     copies = [
@@ -77,7 +74,6 @@
     for one in ins:
         one.start()
     copies[5].start()
-    copies[6].start()
 
     copies[0].wait()
     x = tokens[...]
@@ -112,14 +108,12 @@
                 )
         outs[n].start()
     copies[5].wait()
-    gate = dot32(x, wg[...])
-    copies[6].wait()
     for h in range(heads):
         part = slice(h * value_dim, (h + 1) * value_dim)
         r = readout[:, part]
         scale = lax.rsqrt(jnp.mean(r * r, axis=-1, keepdims=True) + eps_norm)
-        gated_ref[:, part] = (r * scale * gain[...] * jax.nn.silu(gate[:, part])).astype(BF16)
-    rounded = pltpu.make_async_copy(gated_ref, gated_hbm, gated_sem.at[0])
+        normed[:, part] = r * scale * gain[...]
+    rounded = pltpu.make_async_copy(normed, normed_hbm, normed_sem.at[0])
     rounded.start()
     for one in outs:
         one.wait()
@@ -130,7 +124,8 @@
     n_ep,
     n_tp,
     cap,
-    gated_hbm,
+    normed_hbm,
+    wg_hbm,
     wo_hbm,
     tokens_hbm,
     norm_gain_hbm,
@@ -142,7 +137,8 @@
     eu_hbm,
     ed_hbm,
     out_ref,
-    gated,
+    normed,
+    wg,
     wo,
     tokens,
     norm_gain,
@@ -176,10 +172,11 @@
     per_group = router_w.shape[0] // group_w.shape[0]
     slots = n_ep * cap
     operands = [
-        (gated_hbm, gated),
+        (tokens_hbm, tokens),
+        (wg_hbm, wg),
+        (normed_hbm, normed),
         (wo_hbm, wo),
         (routes_hbm, routes),
-        (tokens_hbm, tokens),
         (norm_gain_hbm, norm_gain),
         (norm_bias_hbm, norm_bias),
         (group_w_hbm, group_w),
@@ -223,9 +220,13 @@
 
     loads[0].wait()
     loads[1].wait()
-    part_mine[...] = dot32(gated[...], wo[...]).astype(BF16)
-
+    gate = dot32(tokens[...], wg[...])
     loads[2].wait()
+    gated = (normed[...] * jax.nn.silu(gate)).astype(BF16)
+    loads[3].wait()
+    part_mine[...] = dot32(gated, wo[...]).astype(BF16)
+
+    loads[4].wait()
     first, second = routes[0:1, :], routes[1:2, :]
     before = (
         lax.broadcasted_iota(jnp.int32, (rows, rows), 0)
@@ -245,7 +246,7 @@
     send0, send1 = slot_of(slots, lambda j: j * n_tp + core)
     pick_send = (send0 + send1).astype(BF16)
     back0, back1 = slot_of(slots * n_tp, lambda j: j)
-    for n in range(3, len(loads)):
+    for n in range(5, len(loads)):
         loads[n].wait()
     base = alpha_res * tokens[...].astype(F32) + part_mine[...].astype(F32)
 
@@ -392,7 +393,7 @@
     heads, key_dim, value_dim = recurrent_state.shape[1:]
     in_hbm = pl.BlockSpec(memory_space=pltpu.HBM)
     vmem = pl.BlockSpec(memory_space=pltpu.VMEM)
-    chunk = 2
+    chunk = 1
     chunks = rows // chunk
     dma = pltpu.SemaphoreType.DMA
 
@@ -400,13 +401,13 @@
         return pltpu.VMEM(a.shape, a.dtype)
 
     gain_row = head_gain.reshape(1, value_dim)
-    new_state, gated = pl.pallas_call(
+    new_state, normed = pl.pallas_call(
         functools.partial(attention_kernel, chunk),
         out_shape=(
             jax.ShapeDtypeStruct(recurrent_state.shape, F32),
-            jax.ShapeDtypeStruct((rows, heads * value_dim), BF16),
+            jax.ShapeDtypeStruct((rows, heads * value_dim), F32),
         ),
-        in_specs=[in_hbm] * 8,
+        in_specs=[in_hbm] * 7,
         out_specs=(in_hbm, in_hbm),
         scratch_shapes=[
             like(tokens),
@@ -416,11 +417,10 @@
             like(key_weight),
             like(decay_weight),
             like(value_weight),
-            like(gate_weight),
             like(gain_row),
             pltpu.VMEM((rows, heads * value_dim), F32),
-            pltpu.VMEM((rows, heads * value_dim), BF16),
-            dma((7,)),
+            pltpu.VMEM((rows, heads * value_dim), F32),
+            dma((6,)),
             dma((chunks,)),
             dma((chunks,)),
             dma((1,)),
@@ -434,14 +434,14 @@
         key_weight,
         decay_weight,
         value_weight,
-        gate_weight,
         gain_row,
     )
     experts = router_weight.shape[1]
     cap = 2 * max(1, rows // experts)
     half = width // n_tp
     operands = (
-        gated,
+        normed,
+        gate_weight,
         output_weight,
         tokens,
         norm_gain,

time: 33 us -> 33.6 us (1.018)
  Pallas kernels: 30.7 us -> 31.4 us
    pallas_call x1, Pallas kernels: 7.45 us -> 8.14 us  [on_device(): pl.pallas_call(functools.partial(attention_kernel, chunk), out_shape=(jax...]
where the time goes in v3:
time: 33.6 us; the launch traced here: 33.4 us
  Pallas kernels  31.4 us (93%)
  local copies, waits for them, and re-layouts  1.38 us (4%)
  between operations  0.65 us (2%)
    pallas_call x1, Pallas kernels, on_device(): pl.pallas_call(functools.partial(layer_kernel, n_ep, n_tp, cap), out_shap...  23.3 us
    pallas_call x1, Pallas kernels, on_device(): pl.pallas_call(functools.partial(attention_kernel, chunk), out_shape=(jax...  8.14 us
    unnamed x1, local copies, waits for them, and re-layouts  1.38 us

profile of v3, /device:TPU:0, one launch (start us, length us, event | category | flops | bytes accessed | tf_op | source)
XLA Modules:
  0.0 33.4 jit_solution(11607226475360400783)
XLA Ops:
  0.6 8.1 %attention.1 = (f32[16,2,128,256]{3,2,1,0:T(8,128)}, f32[16,512]{1,0:T(8,128)}) custom-call(bf16[16,2048]{1,0:T(8,128)(2,1)} %tokens_hbm.3, f32[16,2,128,256]{3,2,1,0:T(8,128)} %state_hbm.1, bf16[2048,256]{1,0:T(8,128)(2,1)} %wq_hbm.1, bf16[2048,256]{1,0:T(8,128)(2,1)} %wk_hbm.1, bf16[2048,256]{1,0:T(8,128)(2,1)} %wd_hbm.1, bf16[2048,512]{1,0:T(8,128)(2,1)} %wv_hbm.1, ...), custom_call_target="tpu_custom_call" | custom-call | tf_op jit(solution)/shard_map/attention/pallas_call | solution.py:404
  8.8 23.3 %layer.1 = bf16[16,1024]{1,0:T(8,128)(2,1)} custom-call(f32[16,512]{1,0:T(8,128)} %get-tuple-element.4.normed_hbm, bf16[2048,512]{1,0:T(8,128)(2,1)} %wg_hbm.1, bf16[512,2048]{1,0:T(8,128)(2,1)} %wo_hbm.1, bf16[16,2048]{1,0:T(8,128)(2,1)} %tokens_hbm.3, f32[2,2048]{1,0:T(2,128)} %norm_gain_hbm.1, f32[2,2048]{1,0:T(2,128)} %norm_bias_hbm.1, ...), custom_call_target="tpu_custom_call" | custom-call | tf_op jit(solution)/shard_map/layer/pallas_call | solution.py:456
  32.0 1.4 %copy.20 = bf16[16,1024]{1,0:T(8,128)(2,1)} copy(bf16[16,1024]{1,0:T(8,128)(2,1)} %layer.1) | data formatting | bytes 65536

commit v4 on v2

--- a/solution.py
+++ b/solution.py
@@ -29,7 +29,7 @@
     wg_hbm,
     gain_hbm,
     new_hbm,
-    gated_hbm,
+    gated_ref,
     tokens,
     state,
     fresh,
@@ -40,11 +40,9 @@
     wg,
     gain,
     readout,
-    gated_ref,
     in_sem,
     state_sem,
     out_sem,
-    gated_sem,
 ):
     rows, heads, key_dim, value_dim = state.shape
     chunks = rows // chunk
@@ -119,18 +117,15 @@
         r = readout[:, part]
         scale = lax.rsqrt(jnp.mean(r * r, axis=-1, keepdims=True) + eps_norm)
         gated_ref[:, part] = (r * scale * gain[...] * jax.nn.silu(gate[:, part])).astype(BF16)
-    rounded = pltpu.make_async_copy(gated_ref, gated_hbm, gated_sem.at[0])
-    rounded.start()
     for one in outs:
         one.wait()
-    rounded.wait()
 
 
 def layer_kernel(
     n_ep,
     n_tp,
     cap,
-    gated_hbm,
+    gated,
     wo_hbm,
     tokens_hbm,
     norm_gain_hbm,
@@ -142,7 +137,6 @@
     eu_hbm,
     ed_hbm,
     out_ref,
-    gated,
     wo,
     tokens,
     norm_gain,
@@ -176,7 +170,6 @@
     per_group = router_w.shape[0] // group_w.shape[0]
     slots = n_ep * cap
     operands = [
-        (gated_hbm, gated),
         (wo_hbm, wo),
         (routes_hbm, routes),
         (tokens_hbm, tokens),
@@ -222,10 +215,9 @@
         )
 
     loads[0].wait()
+    part_mine[...] = dot32(gated[...], wo[...]).astype(BF16)
+
     loads[1].wait()
-    part_mine[...] = dot32(gated[...], wo[...]).astype(BF16)
-
-    loads[2].wait()
     first, second = routes[0:1, :], routes[1:2, :]
     before = (
         lax.broadcasted_iota(jnp.int32, (rows, rows), 0)
@@ -245,7 +237,7 @@
     send0, send1 = slot_of(slots, lambda j: j * n_tp + core)
     pick_send = (send0 + send1).astype(BF16)
     back0, back1 = slot_of(slots * n_tp, lambda j: j)
-    for n in range(3, len(loads)):
+    for n in range(2, len(loads)):
         loads[n].wait()
     base = alpha_res * tokens[...].astype(F32) + part_mine[...].astype(F32)
 
@@ -392,12 +384,15 @@
     heads, key_dim, value_dim = recurrent_state.shape[1:]
     in_hbm = pl.BlockSpec(memory_space=pltpu.HBM)
     vmem = pl.BlockSpec(memory_space=pltpu.VMEM)
-    chunk = 2
+    chunk = 4
     chunks = rows // chunk
     dma = pltpu.SemaphoreType.DMA
 
     def like(a):
         return pltpu.VMEM(a.shape, a.dtype)
+
+    def pinned(arrays):
+        return tuple(pltpu.with_memory_space_constraint(a, pltpu.HBM) for a in arrays)
 
     gain_row = head_gain.reshape(1, value_dim)
     new_state, gated = pl.pallas_call(
@@ -407,7 +402,7 @@
             jax.ShapeDtypeStruct((rows, heads * value_dim), BF16),
         ),
         in_specs=[in_hbm] * 8,
-        out_specs=(in_hbm, in_hbm),
+        out_specs=(in_hbm, vmem),
         scratch_shapes=[
             like(tokens),
             like(recurrent_state),
@@ -419,29 +414,30 @@
             like(gate_weight),
             like(gain_row),
             pltpu.VMEM((rows, heads * value_dim), F32),
-            pltpu.VMEM((rows, heads * value_dim), BF16),
             dma((7,)),
             dma((chunks,)),
             dma((chunks,)),
-            dma((1,)),
         ],
-        compiler_params=pltpu.CompilerParams(vmem_limit_bytes=67043328),
+        compiler_params=pltpu.CompilerParams(vmem_limit_bytes=40 * 1024 * 1024),
         name="attention",
     )(
-        tokens,
-        recurrent_state,
-        query_weight,
-        key_weight,
-        decay_weight,
-        value_weight,
-        gate_weight,
-        gain_row,
+        *pinned(
+            (
+                tokens,
+                recurrent_state,
+                query_weight,
+                key_weight,
+                decay_weight,
+                value_weight,
+                gate_weight,
+                gain_row,
+            )
+        )
     )
     experts = router_weight.shape[1]
     cap = 2 * max(1, rows // experts)
     half = width // n_tp
     operands = (
-        gated,
         output_weight,
         tokens,
         norm_gain,
@@ -456,7 +452,7 @@
     new_tokens = pl.pallas_call(
         functools.partial(layer_kernel, n_ep, n_tp, cap),
         out_shape=jax.ShapeDtypeStruct((rows, half), BF16),
-        in_specs=[in_hbm] * len(operands),
+        in_specs=[vmem] + [in_hbm] * len(operands),
         out_specs=vmem,
         scratch_shapes=[like(a) for a in operands]
         + [
@@ -477,10 +473,10 @@
             dma((n_tp, n_ep)),
         ],
         compiler_params=pltpu.CompilerParams(
-            collective_id=0, has_side_effects=True, vmem_limit_bytes=67043328
+            collective_id=0, has_side_effects=True, vmem_limit_bytes=40 * 1024 * 1024
         ),
         name="layer",
-    )(*operands)
+    )(gated, *pinned(operands))
     return new_tokens, new_state
 
 

time: 33 us -> 30.5 us (0.924)
  Pallas kernels: 30.7 us -> 29.1 us
  local copies, waits for them, and re-layouts: 1.38 us -> 0.62 us
    pallas_call x1, Pallas kernels: 7.45 us -> 6.46 us  [on_device(): pl.pallas_call(functools.partial(attention_kernel, chunk), out_shape=(jax...]
    unnamed x1, local copies, waits for them, and re-layouts: 1.38 us -> 0.62 us
    pallas_call x1, Pallas kernels: 23.2 us -> 22.6 us  [on_device(): pl.pallas_call(functools.partial(layer_kernel, n_ep, n_tp, cap), out_shap...]
where the time goes in v4:
time: 30.5 us; the launch traced here: 30.4 us
  Pallas kernels  29.1 us (95%)
  between operations  0.65 us (2%)
  local copies, waits for them, and re-layouts  0.62 us (2%)
    pallas_call x1, Pallas kernels, on_device(): pl.pallas_call(functools.partial(layer_kernel, n_ep, n_tp, cap), out_shap...  22.6 us
    pallas_call x1, Pallas kernels, on_device(): pl.pallas_call(functools.partial(attention_kernel, chunk), out_shape=(jax...  6.46 us
    unnamed x1, local copies, waits for them, and re-layouts  0.62 us

profile of v4, /device:TPU:0, one launch (start us, length us, event | category | flops | bytes accessed | tf_op | source)
XLA Modules:
  0.0 30.4 jit_solution(1792134325441759081)
XLA Ops:
  0.6 6.5 %attention.1 = (f32[16,2,128,256]{3,2,1,0:T(8,128)}, bf16[16,512]{1,0:T(8,128)(2,1)S(1)}) custom-call(bf16[16,2048]{1,0:T(8,128)(2,1)} %tokens_hbm.3, f32[16,2,128,256]{3,2,1,0:T(8,128)} %state_hbm.1, bf16[2048,256]{1,0:T(8,128)(2,1)} %wq_hbm.1, bf16[2048,256]{1,0:T(8,128)(2,1)} %wk_hbm.1, bf16[2048,256]{1,0:T(8,128)(2,1)} %wd_hbm.1, ...), custom_call_target="tpu_custom_call" | custom-call | tf_op jit(solution)/shard_map/attention/pallas_call | solution.py:398
  7.1 22.6 %layer.1 = bf16[16,1024]{1,0:T(8,128)(2,1)S(1)} custom-call(bf16[16,512]{1,0:T(8,128)(2,1)S(1)} %get-tuple-element.4.gated, bf16[512,2048]{1,0:T(8,128)(2,1)} %wo_hbm.1, bf16[16,2048]{1,0:T(8,128)(2,1)} %tokens_hbm.3, f32[2,2048]{1,0:T(2,128)} %norm_gain_hbm.1, f32[2,2048]{1,0:T(2,128)} %norm_bias_hbm.1, bf16[4,2048]{1,0:T(4,128)(2,1)} %bitcast.5, ...), custom_call_target="tpu_custom_call" | custom-call | tf_op jit(solution)/shard_map/layer/pallas_call | solution.py:452
  29.7 0.6 %copy.20 = bf16[16,1024]{1,0:T(8,128)(2,1)} copy(bf16[16,1024]{1,0:T(8,128)(2,1)S(1)} %layer.1) | data formatting | bytes 65536
